TPU v7x, 32 devices: a whole 2x2x4 slice. The times are simulated.
32 devices in a mesh: ra: 8 (over z, y), cb: 4 (over x, core).
Axes of the slice: x: 2, y: 2, z: 4, core: 2. Of those that a mesh axis runs over, the one named last changes fastest.
Arguments:
- tokens: bfloat16 [4, 128, 4096], P(None, None, 'ra'), may hold values from -64 to 64
- norm_gain: float32 [2, 4096], P(None, 'ra'), may hold values from 0.1 to 1.9
- gate_weight: bfloat16 [2, 4096, 11264], P(None, 'ra', 'cb'), may hold values from -0.09375 to 0.09375
- up_weight: bfloat16 [2, 4096, 11264], P(None, 'ra', 'cb'), may hold values from -0.09375 to 0.09375
- gate_taps: float32 [2, 3, 11264], P(None, None, 'cb'), may hold values from -3 to 3
- up_taps: float32 [2, 3, 11264], P(None, None, 'cb'), may hold values from -3 to 3
- gate_bias: float32 [2, 11264], P(None, 'cb'), may hold values from -3 to 3
- up_bias: float32 [2, 11264], P(None, 'cb'), may hold values from -3 to 3
- down_weight: bfloat16 [2, 11264, 4096], P(None, 'cb', 'ra'), may hold values from -0.0546875 to 0.0546875
Outputs:
- mixed: bfloat16 [4, 128, 4096], P(None, None, 'ra')
All inputs are finite; a program needn't handle non-finite values.
Results may differ from a plain program's by a relative error of at most 0.03.
Values may be sent and summed in bfloat16 or wider, within the bound.
A program may use at most 64 MiB of HBM per device.

v0:
```python
import jax
import jax.numpy as jnp
from jax import lax
from jax.sharding import PartitionSpec as P

D = 4096
KERNEL = 3
LAYERS = 2
eps = 1e-06
resid_scale = 0.5


def causal_conv(projected, kernel, offsets, seqs, length):
    values = projected.astype(jnp.float32).reshape(seqs, length, 2, projected.shape[2])
    padded = jnp.pad(values, ((0, 0), (KERNEL - 1, 0), (0, 0), (0, 0)))
    result = offsets
    for tap_idx in range(KERNEL):
        result = result + kernel[tap_idx] * padded[:, tap_idx : tap_idx + length]
    return result.reshape(seqs * length, 2, projected.shape[2])


def per_device(
    tokens, norm_gain, gate_weight, up_weight, gate_taps, up_taps, gate_bias, up_bias, down_weight
):
    seqs, length, width_local = tokens.shape
    rows_count = seqs * length
    carried = tokens.reshape(rows_count, width_local).astype(jnp.float32)
    for layer_idx in range(LAYERS):
        local_squares = jnp.sum(carried * carried, axis=1)
        scaled = (carried * norm_gain[layer_idx]).astype(jnp.bfloat16)
        kernel = jnp.stack([gate_taps[layer_idx], up_taps[layer_idx]], axis=1)
        offsets = jnp.stack([gate_bias[layer_idx], up_bias[layer_idx]], axis=0)
        down_local = down_weight[layer_idx]
        partial_value = jnp.stack(
            [
                jnp.dot(scaled, gate_weight[layer_idx], preferred_element_type=jnp.float32),
                jnp.dot(scaled, up_weight[layer_idx], preferred_element_type=jnp.float32),
            ],
            axis=1,
        )
        row_squares = lax.psum(local_squares, "ra")
        summed = lax.psum(partial_value.astype(jnp.bfloat16), "ra").astype(jnp.float32)
        inverse = lax.rsqrt(row_squares / D + eps)
        projected = (summed * inverse[:, None, None]).astype(jnp.bfloat16)
        convolved = causal_conv(projected, kernel, offsets, seqs, length)
        hidden = (jax.nn.silu(convolved[:, 0]) * convolved[:, 1]).astype(jnp.bfloat16)
        branch_part = jnp.dot(hidden, down_local, preferred_element_type=jnp.float32)
        branch = lax.psum(branch_part.astype(jnp.bfloat16), "cb").astype(jnp.float32)
        carried = resid_scale * carried + branch
    return carried.astype(jnp.bfloat16).reshape(seqs, length, width_local)


def solution(mesh):
    in_specs = (
        P(None, None, "ra"),
        P(None, "ra"),
        P(None, "ra", "cb"),
        P(None, "ra", "cb"),
        P(None, None, "cb"),
        P(None, None, "cb"),
        P(None, "cb"),
        P(None, "cb"),
        P(None, "cb", "ra"),
    )
    out_specs = P(None, None, "ra")
    return jax.shard_map(
        per_device, mesh=mesh, in_specs=in_specs, out_specs=out_specs, check_vma=False
    )
```

profile of v0, /device:TPU:0, one launch (start us, length us, event | category | flops | bytes accessed | tf_op | source)
XLA Modules:
  0.0 539.4 jit_solution(4109739938134989243)
XLA Ops:
  6.5 0.0 all-reduce.7.cloned.1.call-start
  6.5 0.0 copy-start.5
  6.5 0.9 fusion.60
  7.4 1.5 convert_multiply_fusion.2
  8.9 3.5 fusion.13
  12.3 0.0 copy-done.5
  12.4 1.7 fusion.12
  14.0 3.0 pad_maximum_fusion
  17.1 0.0 copy-start.3
  17.1 0.0 copy-start.4
  17.1 0.0 copy-start.1
  17.1 0.0 copy-start.2
  17.1 0.0 all-reduce.7.cloned.1.call-update
  17.1 0.0 all-reduce.9.cloned.1.call-start
  17.1 24.1 %psum.43 = f32[512]{0:T(512)S(1)} all-reduce(f32[512]{0:T(512)S(1)} %bitcast.89), channel_id=1, replica_groups=mesh['ra'=8,'cb'=4] {'ra'}, use_global_device_ids=true, to_apply=%region_2.0 | all-reduce | flops 512 | bytes 4096 | tf_op jit(solution)/shard_map/psum | solution.py:41
  41.2 0.0 copy-done.3
  41.3 0.0 copy-done.4
  41.4 0.0 copy-done.1
  41.4 0.0 copy-done.2
  41.4 0.1 slice_bitcast_fusion
  41.5 0.1 fusion.52
  41.6 177.0 %all-reduce.7.cloned.1.call-done = bf16[512,2,2816]{2,0,1:T(8,128)(2,1)} async-done(((bf16[512,2,2816]{2,0,1:T(8,128)(2,1)}), bf16[512,2,2816]{2,0,1:T(8,128)(2,1)}) %all-reduce.7.cloned.1.call-update) | async-done | bytes 5767184 | tf_op jit(solution)/shard_map/psum | solution.py:42
  218.5 4.2 multiply_convert_fusion.1
  222.7 0.0 slice-start
  222.8 1.0 convert.22
  223.8 0.0 slice-start.1
  223.8 6.3 %fusion.3 = f32[4,128,2,2816]{3,1,0,2:T(8,128)} fusion(f32[4,128,2,2816]{3,1,0,2:T(8,128)S(1)} %convert.22, f32[2,2816]{1,0:T(2,128)S(1)} %get-tuple-element.18, f32[2,2816]{1,0:T(2,128)S(1)} %get-tuple-element.19, f32[2,2816]{1,0:T(2,128)S(1)} %get-tuple-element.17, f32[2,2816]{1,0:T(2,128)S(1)} %get-tuple-element.28), kind=kLoop, calls=%fused_computation.7 | loop fusion | flops 17301504 | bytes 23158784 | tf_op jit(solution)/shard_map/add | solution.py:18
  230.1 0.0 slice-done
  230.1 0.0 slice-done.1
  230.1 6.9 %fusion.34 = bf16[512,512]{1,0:T(8,128)(2,1)} fusion(bf16[2,2816,512]{2,1,0:T(8,128)(2,1)S(1)} %bitcast.93, f32[512,2,2816]{2,0,1:T(8,128)} %bitcast.85), kind=kOutput, calls=%fused_computation.49 | convolution fusion | flops 1485307904 | bytes 14942208 | tf_op jit(solution)/shard_map/dot_general | solution.py:47
  237.0 0.0 all-reduce.9.cloned.1.call-update
  237.0 0.2 all-reduce.11.cloned.1.call-start
  237.3 32.3 %all-reduce.9.cloned.1.call-done = bf16[512,512]{1,0:T(8,128)(2,1)} async-done(((bf16[512,512]{1,0:T(8,128)(2,1)}), bf16[512,512]{1,0:T(8,128)(2,1)}) %all-reduce.9.cloned.1.call-update) | async-done | bytes 524304 | tf_op jit(solution)/shard_map/psum | solution.py:48
  269.6 1.3 multiply_reduce_fusion
  270.9 3.5 fusion.15
  274.4 3.5 fusion.14
  277.9 3.0 pad_maximum_fusion.1
  280.9 0.0 all-reduce.11.cloned.1.call-update
  280.9 0.0 all-reduce.13.cloned.1.call-start
  281.0 0.1 fusion.54
  281.0 22.5 %psum.46 = f32[512]{0:T(512)S(1)} all-reduce(f32[512]{0:T(512)S(1)} %get-tuple-element.5), channel_id=1, replica_groups=mesh['ra'=8,'cb'=4] {'ra'}, use_global_device_ids=true, to_apply=%region_6.7 | all-reduce | flops 512 | bytes 4096 | tf_op jit(solution)/shard_map/psum | solution.py:41
  303.5 176.2 %all-reduce.11.cloned.1.call-done = bf16[512,2,2816]{2,0,1:T(8,128)(2,1)} async-done(((bf16[512,2,2816]{2,0,1:T(8,128)(2,1)}), bf16[512,2,2816]{2,0,1:T(8,128)(2,1)}) %all-reduce.11.cloned.1.call-update) | async-done | bytes 5767184 | tf_op jit(solution)/shard_map/psum | solution.py:42
  479.7 4.2 multiply_convert_fusion
  483.9 0.0 slice-start.2
  483.9 1.0 convert.23
  484.9 0.0 slice-start.3
  485.0 6.3 %fusion.8 = f32[4,128,2,2816]{3,1,0,2:T(8,128)} fusion(f32[4,128,2,2816]{3,1,0,2:T(8,128)S(1)} %convert.23, f32[2,2816]{1,0:T(2,128)S(1)} %get-tuple-element.11, f32[2,2816]{1,0:T(2,128)S(1)} %get-tuple-element.12, f32[2,2816]{1,0:T(2,128)S(1)} %get-tuple-element.10, f32[2,2816]{1,0:T(2,128)S(1)} %get-tuple-element.29), kind=kLoop, calls=%fused_computation.12 | loop fusion | flops 17301504 | bytes 23158784 | tf_op jit(solution)/shard_map/add | solution.py:18
  491.2 0.0 slice-done.2
  491.2 0.0 slice-done.3
  491.2 0.0 copy-start
  491.2 7.0 %fusion.39 = bf16[512,512]{1,0:T(8,128)(2,1)} fusion(bf16[2,2816,512]{2,1,0:T(8,128)(2,1)S(1)} %bitcast.95, f32[512,2,2816]{2,0,1:T(8,128)} %bitcast.86), kind=kOutput, calls=%fused_computation.50 | convolution fusion | flops 1485307904 | bytes 14942208 | tf_op jit(solution)/shard_map/dot_general | solution.py:47
  498.2 0.0 all-reduce.13.cloned.1.call-update
  498.3 32.5 %all-reduce.13.cloned.1.call-done = bf16[512,512]{1,0:T(8,128)(2,1)} async-done(((bf16[512,512]{1,0:T(8,128)(2,1)}), bf16[512,512]{1,0:T(8,128)(2,1)}) %all-reduce.13.cloned.1.call-update) | async-done | bytes 524304 | tf_op jit(solution)/shard_map/psum | solution.py:48
  530.8 0.0 copy-done
  530.8 2.0 add_convert_fusion
  (7 shorter events, 0.1 us)
Async XLA Ops:
  6.5 212.0 %all-reduce.7.cloned.1.call-start = ((), (), s32[]{:S(2)}) async-start(), calls=%async_computation | async-start | bytes 11534336 | tf_op jit(solution)/shard_map/psum | solution.py:42
  6.5 5.8 %copy-start.5 = (bf16[2,512,2816]{2,1,0:T(8,128)(2,1)S(1)}, bf16[2,512,2816]{2,1,0:T(8,128)(2,1)}, u32[]{:S(2)}) copy-start(bf16[2,512,2816]{2,1,0:T(8,128)(2,1)} %param.11) | copy-start | bytes 17301508
  17.1 24.2 %copy-start.3 = (f32[2,2816]{1,0:T(2,128)S(1)}, f32[2,2816]{1,0:T(2,128)}, u32[]{:S(2)}) copy-start(f32[2,2816]{1,0:T(2,128)} %param.15) | copy-start | bytes 67588
  17.1 24.2 %copy-start.4 = (f32[2,2816]{1,0:T(2,128)S(1)}, f32[2,2816]{1,0:T(2,128)}, u32[]{:S(2)}) copy-start(f32[2,2816]{1,0:T(2,128)} %param.16) | copy-start | bytes 67588
  17.1 24.3 %copy-start.1 = (f32[2,3,2816]{2,0,1:T(2,128)S(1)}, f32[2,3,2816]{2,0,1:T(2,128)}, u32[]{:S(2)}) copy-start(f32[2,3,2816]{2,0,1:T(2,128)} %param.14) | copy-start | bytes 202756
  17.1 24.3 %copy-start.2 = (f32[2,3,2816]{2,0,1:T(2,128)S(1)}, f32[2,3,2816]{2,0,1:T(2,128)}, u32[]{:S(2)}) copy-start(f32[2,3,2816]{2,0,1:T(2,128)} %param.13) | copy-start | bytes 202756
  17.1 252.5 %all-reduce.9.cloned.1.call-start = ((), (), s32[]{:S(2)}) async-start(), calls=%async_computation.1 | async-start | bytes 1048576 | tf_op jit(solution)/shard_map/psum | solution.py:48
  222.7 7.3 %slice-start = ((s8[5767168]{0:T(1024)(128)(4,1)}), s8[1572864]{0:T(1024)(128)(4,1)S(1)}, s32[]{:S(2)}) async-start(s8[5767168]{0:T(1024)(128)(4,1)} %bitcast.92), calls=%async_computation.4 | async-start | bytes 3145728
  223.8 6.3 %slice-start.1 = ((s8[5767168]{0:T(1024)(128)(4,1)}), s8[4194304]{0:T(1024)(128)(4,1)S(1)}, s32[]{:S(2)}) async-start(s8[5767168]{0:T(1024)(128)(4,1)} %bitcast.92), calls=%async_computation.5 | async-start | bytes 8388608
  237.0 242.6 %all-reduce.11.cloned.1.call-start = ((), (), s32[]{:S(2)}) async-start(), calls=%async_computation.2 | async-start | bytes 11534336 | tf_op jit(solution)/shard_map/psum | solution.py:42
  280.9 249.9 %all-reduce.13.cloned.1.call-start = ((), (), s32[]{:S(2)}) async-start(), calls=%async_computation.3 | async-start | bytes 1048576 | tf_op jit(solution)/shard_map/psum | solution.py:48
  483.9 7.3 %slice-start.2 = ((s8[5767168]{0:T(1024)(128)(4,1)}), s8[1572864]{0:T(1024)(128)(4,1)S(1)}, s32[]{:S(2)}) async-start(s8[5767168]{0:T(1024)(128)(4,1)} %bitcast.94), calls=%async_computation.6 | async-start | bytes 3145728
  484.9 6.3 %slice-start.3 = ((s8[5767168]{0:T(1024)(128)(4,1)}), s8[4194304]{0:T(1024)(128)(4,1)S(1)}, s32[]{:S(2)}) async-start(s8[5767168]{0:T(1024)(128)(4,1)} %bitcast.94), calls=%async_computation.7 | async-start | bytes 8388608
  491.2 39.5 %copy-start = (bf16[512,512]{1,0:T(8,128)(2,1)S(1)}, bf16[512,512]{1,0:T(8,128)(2,1)}, u32[]{:S(2)}) copy-start(bf16[512,512]{1,0:T(8,128)(2,1)} %all-reduce.9.cloned.1.call-done) | copy-start | bytes 1572868
Sparse Core Ops, SparseCore 0:
  17.2 201.2 all-reduce.6
  237.2 32.3 all-reduce.8
  281.0 198.6 all-reduce.10
  498.4 32.3 all-reduce.12
where the time goes:
time: 540 us; the launch traced here: 539 us
  waiting for transfers between devices  418 us (77%)
  blocking collectives  46.6 us (9%)
  other arithmetic  34.1 us (6%)
  matrix products  26 us (5%)
  between operations  13.3 us (2%)
    psum x2, waiting for transfers between devices, per_device(): lax.psum(partial_value.astype(jnp.bfloat16), 'ra').astype(jnp.float32)  353 us
    psum x2, waiting for transfers between devices, per_device(): lax.psum(branch_part.astype(jnp.bfloat16), 'cb').astype(jnp.float32)  64.8 us
    psum x2, blocking collectives, per_device(): row_squares = lax.psum(local_squares, 'ra')  46.6 us
    dot_general x2, matrix products, per_device(): jnp.dot(hidden, down_local, preferred_element_type=jnp.float32)  13.9 us
    add x2, other arithmetic, causal_conv(): result = result + kernel[tap_idx] * padded[:, tap_idx:tap_idx + length]  12.6 us
  transfers between devices with their start and end apart: 4, of which 4 were waited for; matrix products, arithmetic and copies ran while one was open for 0% of the time, Pallas kernels for 0%

commit v1 on v0

--- a/solution.py
+++ b/solution.py
@@ -38,7 +38,11 @@
             ],
             axis=1,
         )
-        row_squares = lax.psum(local_squares, "ra")
+        row_squares = local_squares
+        for hop in (1, 2, 4):
+            row_squares = row_squares + lax.ppermute(
+                row_squares, "ra", [(dev, dev ^ hop) for dev in range(8)]
+            )
         summed = lax.psum(partial_value.astype(jnp.bfloat16), "ra").astype(jnp.float32)
         inverse = lax.rsqrt(row_squares / D + eps)
         projected = (summed * inverse[:, None, None]).astype(jnp.bfloat16)

time: 540 us -> 539 us (level)
  blocking collectives: 46.6 us -> 0 us
  waiting for transfers between devices: 418 us -> 451 us
  starting transfers between devices: 0.31 us -> 13.9 us
    psum x2 -> x0, blocking collectives: 46.6 us -> none  [per_device(): row_squares = lax.psum(local_squares, 'ra')]
    psum x2, waiting for transfers between devices: 353 us -> 373 us  [per_device(): lax.psum(partial_value.astype(jnp.bfloat16), 'ra').astype(jnp.float32)]
    ppermute x0 -> x6, starting transfers between devices: none -> 13.6 us  [per_device(): lax.ppermute(row_squares, 'ra', [(dev, dev ^ hop) for dev in range(8)])]
    ppermute x0 -> x6, waiting for transfers between devices: none -> 13 us  [per_device(): lax.ppermute(row_squares, 'ra', [(dev, dev ^ hop) for dev in range(8)])]
  transfers between devices with their start and end apart: 4 -> 10, of which waited for: 4 -> 10; matrix products, arithmetic and copies ran while one was open for 0% -> 0% of each run, Pallas kernels for 0% -> 0%
where the time goes in v1:
time: 539 us
  waiting for transfers between devices  451 us (84%)
  other arithmetic  33.9 us (6%)
  matrix products  26 us (5%)
  starting transfers between devices  13.9 us (3%)
  between operations  13.3 us (2%)
    psum x2, waiting for transfers between devices, per_device(): lax.psum(partial_value.astype(jnp.bfloat16), 'ra').astype(jnp.float32)  373 us
    psum x2, waiting for transfers between devices, per_device(): lax.psum(branch_part.astype(jnp.bfloat16), 'cb').astype(jnp.float32)  64.8 us
    dot_general x2, matrix products, per_device(): jnp.dot(hidden, down_local, preferred_element_type=jnp.float32)  13.9 us
    ppermute x6, starting transfers between devices, per_device(): lax.ppermute(row_squares, 'ra', [(dev, dev ^ hop) for dev in range(8)])  13.6 us
    ppermute x6, waiting for transfers between devices, per_device(): lax.ppermute(row_squares, 'ra', [(dev, dev ^ hop) for dev in range(8)])  13 us
    add x2, other arithmetic, causal_conv(): result = result + kernel[tap_idx] * padded[:, tap_idx:tap_idx + length]  12.4 us
  transfers between devices with their start and end apart: 10, of which 10 were waited for; matrix products, arithmetic and copies ran while one was open for 0% of the time, Pallas kernels for 0%

profile of v1, /device:TPU:0, one launch (start us, length us, event | category | flops | bytes accessed | tf_op | source)
XLA Modules:
  0.0 538.8 jit_solution(3745252764109744123)
XLA Ops:
  6.5 0.0 all-reduce.7.cloned.1.call-start
  6.5 0.0 copy-start.5
  6.5 0.9 fusion.60
  7.4 1.5 convert_multiply_fusion.2
  8.9 3.5 fusion.13
  12.3 0.0 copy-done.5
  12.4 1.7 fusion.12
  14.0 3.0 pad_maximum_fusion
  17.1 0.0 copy-start.3
  17.1 0.0 copy-start.1
  17.1 0.0 copy-start.2
  17.1 0.0 copy-start.4
  17.1 0.0 all-reduce.7.cloned.1.call-update
  17.1 0.0 all-reduce.9.cloned.1.call-start
  17.1 3.1 collective-permute-start
  20.2 0.0 copy-done.3
  20.2 0.0 copy-done.1
  20.2 0.0 copy-done.2
  20.2 0.1 slice_bitcast_fusion
  20.4 0.0 copy-done.4
  20.4 1.4 collective-permute-done
  21.8 2.1 collective-permute-start.1
  23.8 0.1 fusion.52
  23.9 1.5 collective-permute-done.1
  25.4 3.0 collective-permute-start.2
  28.5 3.4 collective-permute-done.2
  31.9 186.4 %all-reduce.7.cloned.1.call-done = bf16[512,2,2816]{2,0,1:T(8,128)(2,1)} async-done(((bf16[512,2,2816]{2,0,1:T(8,128)(2,1)}), bf16[512,2,2816]{2,0,1:T(8,128)(2,1)}) %all-reduce.7.cloned.1.call-update) | async-done | bytes 5767184 | tf_op jit(solution)/shard_map/psum | solution.py:46
  218.3 4.2 multiply_convert_fusion.1
  222.5 0.0 slice-start
  222.5 1.0 convert.22
  223.6 0.0 slice-start.1
  223.6 6.2 %fusion.3 = f32[4,128,2,2816]{3,1,0,2:T(8,128)} fusion(f32[4,128,2,2816]{3,1,0,2:T(8,128)S(1)} %convert.22, f32[2,2816]{1,0:T(2,128)S(1)} %get-tuple-element.18, f32[2,2816]{1,0:T(2,128)S(1)} %get-tuple-element.19, f32[2,2816]{1,0:T(2,128)S(1)} %get-tuple-element.17, f32[2,2816]{1,0:T(2,128)S(1)} %get-tuple-element.28), kind=kLoop, calls=%fused_computation.7 | loop fusion | flops 17301504 | bytes 23158784 | tf_op jit(solution)/shard_map/add | solution.py:18
  229.8 0.0 slice-done
  229.8 0.0 slice-done.1
  229.8 6.9 %fusion.34 = bf16[512,512]{1,0:T(8,128)(2,1)} fusion(bf16[2,2816,512]{2,1,0:T(8,128)(2,1)S(1)} %bitcast.94, f32[512,2,2816]{2,0,1:T(8,128)} %bitcast.86), kind=kOutput, calls=%fused_computation.49 | convolution fusion | flops 1485307904 | bytes 14942208 | tf_op jit(solution)/shard_map/dot_general | solution.py:51
  236.7 0.0 all-reduce.9.cloned.1.call-update
  236.7 0.2 all-reduce.11.cloned.1.call-start
  237.0 32.3 %all-reduce.9.cloned.1.call-done = bf16[512,512]{1,0:T(8,128)(2,1)} async-done(((bf16[512,512]{1,0:T(8,128)(2,1)}), bf16[512,512]{1,0:T(8,128)(2,1)}) %all-reduce.9.cloned.1.call-update) | async-done | bytes 524304 | tf_op jit(solution)/shard_map/psum | solution.py:52
  269.3 1.3 multiply_reduce_fusion
  270.6 3.5 fusion.15
  274.1 3.5 fusion.14
  277.6 3.0 pad_maximum_fusion.1
  280.6 0.0 all-reduce.11.cloned.1.call-update
  280.6 0.0 all-reduce.13.cloned.1.call-start
  280.7 1.5 collective-permute-start.3
  282.2 2.1 collective-permute-done.3
  284.3 1.5 collective-permute-start.4
  285.8 2.1 collective-permute-done.4
  287.9 2.4 collective-permute-start.5
  290.3 0.1 fusion.54
  290.4 2.5 collective-permute-done.5
  292.9 186.3 %all-reduce.11.cloned.1.call-done = bf16[512,2,2816]{2,0,1:T(8,128)(2,1)} async-done(((bf16[512,2,2816]{2,0,1:T(8,128)(2,1)}), bf16[512,2,2816]{2,0,1:T(8,128)(2,1)}) %all-reduce.11.cloned.1.call-update) | async-done | bytes 5767184 | tf_op jit(solution)/shard_map/psum | solution.py:46
  479.2 4.2 multiply_convert_fusion
  483.4 0.0 slice-start.2
  483.4 1.0 convert.23
  484.5 0.0 slice-start.3
  484.5 6.2 %fusion.8 = f32[4,128,2,2816]{3,1,0,2:T(8,128)} fusion(f32[4,128,2,2816]{3,1,0,2:T(8,128)S(1)} %convert.23, f32[2,2816]{1,0:T(2,128)S(1)} %get-tuple-element.11, f32[2,2816]{1,0:T(2,128)S(1)} %get-tuple-element.12, f32[2,2816]{1,0:T(2,128)S(1)} %get-tuple-element.10, f32[2,2816]{1,0:T(2,128)S(1)} %get-tuple-element.29), kind=kLoop, calls=%fused_computation.12 | loop fusion | flops 17301504 | bytes 23158784 | tf_op jit(solution)/shard_map/add | solution.py:18
  490.7 0.0 slice-done.2
  490.7 0.0 slice-done.3
  490.7 7.0 %fusion.39 = bf16[512,512]{1,0:T(8,128)(2,1)} fusion(bf16[2,2816,512]{2,1,0:T(8,128)(2,1)S(1)} %bitcast.96, f32[512,2,2816]{2,0,1:T(8,128)} %bitcast.87), kind=kOutput, calls=%fused_computation.50 | convolution fusion | flops 1485307904 | bytes 14942208 | tf_op jit(solution)/shard_map/dot_general | solution.py:51
  497.7 0.0 all-reduce.13.cloned.1.call-update
  497.7 32.5 %all-reduce.13.cloned.1.call-done = bf16[512,512]{1,0:T(8,128)(2,1)} async-done(((bf16[512,512]{1,0:T(8,128)(2,1)}), bf16[512,512]{1,0:T(8,128)(2,1)}) %all-reduce.13.cloned.1.call-update) | async-done | bytes 524304 | tf_op jit(solution)/shard_map/psum | solution.py:52
  530.2 0.0 copy-done
  530.2 2.0 add_convert_fusion
  (12 shorter events, 0.1 us)
Async XLA Ops:
  6.5 211.8 %all-reduce.7.cloned.1.call-start = ((), (), s32[]{:S(2)}) async-start(), calls=%async_computation | async-start | bytes 11534336 | tf_op jit(solution)/shard_map/psum | solution.py:46
  6.5 5.8 %copy-start.5 = (bf16[2,512,2816]{2,1,0:T(8,128)(2,1)S(1)}, bf16[2,512,2816]{2,1,0:T(8,128)(2,1)}, u32[]{:S(2)}) copy-start(bf16[2,512,2816]{2,1,0:T(8,128)(2,1)} %param.11) | copy-start | bytes 17301508
  17.1 3.1 copy-start.3
  17.1 3.2 copy-start.1
  17.1 3.2 copy-start.2
  17.1 3.3 copy-start.4
  17.1 252.2 %all-reduce.9.cloned.1.call-start = ((), (), s32[]{:S(2)}) async-start(), calls=%async_computation.1 | async-start | bytes 1048576 | tf_op jit(solution)/shard_map/psum | solution.py:52
  17.1 4.6 collective-permute-start
  21.8 3.6 collective-permute-start.1
  25.4 6.5 %collective-permute-start.2 = (f32[512]{0:T(512)S(1)}, f32[512]{0:T(512)S(1)}, u32[]{:S(2)}, u32[]{:S(2)}) collective-permute-start(f32[512]{0:T(512)S(1)} %add.81), channel_id=1, source_target_pairs={{0,16},{4,20},{8,24},{12,28},{16,0},{20,4},{24,8},{28,12},{1,17},{... | collective-permute-start | bytes 6152 | tf_op jit(solution)/shard_map/ppermute | solution.py:43
  222.5 7.3 %slice-start = ((s8[5767168]{0:T(1024)(128)(4,1)}), s8[1572864]{0:T(1024)(128)(4,1)S(1)}, s32[]{:S(2)}) async-start(s8[5767168]{0:T(1024)(128)(4,1)} %bitcast.93), calls=%async_computation.4 | async-start | bytes 3145728
  223.6 6.2 %slice-start.1 = ((s8[5767168]{0:T(1024)(128)(4,1)}), s8[4194304]{0:T(1024)(128)(4,1)S(1)}, s32[]{:S(2)}) async-start(s8[5767168]{0:T(1024)(128)(4,1)} %bitcast.93), calls=%async_computation.5 | async-start | bytes 8388608
  236.7 242.5 %all-reduce.11.cloned.1.call-start = ((), (), s32[]{:S(2)}) async-start(), calls=%async_computation.2 | async-start | bytes 11534336 | tf_op jit(solution)/shard_map/psum | solution.py:46
  280.6 249.6 %all-reduce.13.cloned.1.call-start = ((), (), s32[]{:S(2)}) async-start(), calls=%async_computation.3 | async-start | bytes 1048576 | tf_op jit(solution)/shard_map/psum | solution.py:52
  280.7 3.7 collective-permute-start.3
  284.3 3.6 collective-permute-start.4
  287.9 5.0 collective-permute-start.5
  483.4 7.3 %slice-start.2 = ((s8[5767168]{0:T(1024)(128)(4,1)}), s8[1572864]{0:T(1024)(128)(4,1)S(1)}, s32[]{:S(2)}) async-start(s8[5767168]{0:T(1024)(128)(4,1)} %bitcast.95), calls=%async_computation.6 | async-start | bytes 3145728
  484.5 6.2 %slice-start.3 = ((s8[5767168]{0:T(1024)(128)(4,1)}), s8[4194304]{0:T(1024)(128)(4,1)S(1)}, s32[]{:S(2)}) async-start(s8[5767168]{0:T(1024)(128)(4,1)} %bitcast.95), calls=%async_computation.7 | async-start | bytes 8388608
  490.7 39.5 %copy-start = (bf16[512,512]{1,0:T(8,128)(2,1)S(1)}, bf16[512,512]{1,0:T(8,128)(2,1)}, u32[]{:S(2)}) copy-start(bf16[512,512]{1,0:T(8,128)(2,1)} %all-reduce.9.cloned.1.call-done) | copy-start | bytes 1572868
Sparse Core Ops, SparseCore 0:
  17.2 201.0 all-reduce.6
  236.9 32.3 all-reduce.8
  280.7 198.4 all-reduce.10
  497.8 32.3 all-reduce.12
